TPU v7x, 32 devices: a whole 2x2x4 slice. The times are simulated.
32 devices in a mesh: ep: 16 (over z, y, x), tp: 2 (over core).
Axes of the slice: x: 2, y: 2, z: 4, core: 2. Of those that a mesh axis runs over, the one named last changes fastest.
Arguments:
- tokens: bfloat16 [64, 4096], P('ep'), may hold values from -6 to 6
- memory: float32 [64, 8, 256, 512], P('ep', 'tp'), may hold values from -6 to 6
- normalizer: float32 [64, 8, 256], P('ep', 'tp'), may hold values from -6 to 6
- stabilizer: float32 [64, 8], P('ep', 'tp'), may hold values from -4 to 4
- norm_gain: float32 [4096], replicated, may hold values from 0.1 to 1.9
- w_query: bfloat16 [4096, 8, 256], P(None, 'tp', 'ep'), may hold values from -0.09375 to 0.09375
- w_key: bfloat16 [4096, 8, 256], P(None, 'tp', 'ep'), may hold values from -0.09375 to 0.09375
- w_value: bfloat16 [4096, 8, 512], P(None, 'tp', 'ep'), may hold values from -0.09375 to 0.09375
- w_outgate: bfloat16 [4096, 8, 512], P(None, 'tp', 'ep'), may hold values from -0.09375 to 0.09375
- w_input: bfloat16 [4096, 8], P(None, 'tp'), may hold values from -0.09375 to 0.09375
- w_forget: bfloat16 [4096, 8], P(None, 'tp'), may hold values from -0.09375 to 0.09375
- forget_bias: float32 [8], P('tp'), may hold values from 0 to 4
- w_out: bfloat16 [4096, 4096], P('tp', 'ep'), may hold values from -0.09375 to 0.09375
- ffn_gain: float32 [4096], replicated, may hold values from 0.1 to 1.9
- w_gate: bfloat16 [16, 4096, 512], P('ep', None, 'tp'), may hold values from -0.09375 to 0.09375
- w_up: bfloat16 [16, 4096, 512], P('ep', None, 'tp'), may hold values from -0.09375 to 0.09375
- w_down: bfloat16 [16, 512, 4096], P('ep', 'tp'), may hold values from -0.25 to 0.25
- expert_ids: int32 [64, 2], P('ep'), may hold values from 0 to 15, as said below
- route_weights: float32 [64, 2], P('ep'), may hold values from 0.1 to 1
Outputs:
- out: bfloat16 [64, 4096], P('ep')
- memory_next: float32 [64, 8, 256, 512], P('ep', 'tp')
- normalizer_next: float32 [64, 8, 256], P('ep', 'tp')
- stabilizer_next: float32 [64, 8], P('ep', 'tp')
Inputs may be any that keep to these rules, and one draw needn't show every extreme that they name: `expert_ids`: the 2 experts of a token differ and lie in one group of 8 consecutive experts. Beyond that, any choice is allowed: for instance, all 4 tokens of one index of ep may name the same expert.
All inputs are finite; a program needn't handle non-finite values.
Results may differ from a plain program's by a relative error of at most 0.013.
Values may be sent and summed in bfloat16 or wider, within the bound.
No kernel may reach another device: no remote copies, remote signals or barrier semaphores. Data moves between devices by JAX's collectives and lax.ppermute only.
A program may use at most 128 MiB of HBM per device.

v0:
```python
import jax
import jax.numpy as jnp
from jax import lax
from jax.sharding import PartitionSpec as P


def rms_scale(values, gain):
    return values * lax.rsqrt(jnp.mean(values * values, axis=-1, keepdims=True) + 1e-06) * gain


def product(left, right):
    return jnp.dot(left, right, preferred_element_type=jnp.float32)


def rounded_term(values):
    return lax.optimization_barrier(values.astype(jnp.bfloat16)).astype(jnp.float32)


def body(
    tokens,
    memory,
    normalizer,
    stabilizer,
    norm_gain,
    w_query,
    w_key,
    w_value,
    w_outgate,
    w_input,
    w_forget,
    forget_bias,
    w_out,
    ffn_gain,
    w_gate,
    w_up,
    w_down,
    expert_ids,
    route_weights,
):
    seqs, width = tokens.shape
    heads, key_size, value_size = (memory.shape[1], memory.shape[2], memory.shape[3])
    value_width = heads * value_size
    key_piece = w_query.shape[2]
    value_piece = w_value.shape[2]
    query_cols = w_query.reshape(width, heads * key_piece)
    key_cols = w_key.reshape(width, heads * key_piece)
    value_cols = w_value.reshape(width, heads * value_piece)
    outgate_cols = w_outgate.reshape(width, heads * value_piece)
    normed = rms_scale(tokens.astype(jnp.float32), norm_gain).astype(jnp.bfloat16)
    piece = lax.all_gather(normed, "ep", axis=0, tiled=True)
    projected = jnp.concatenate(
        [
            product(piece, query_cols),
            product(piece, key_cols),
            product(piece, value_cols),
            product(piece, outgate_cols),
        ],
        axis=1,
    ).astype(jnp.bfloat16)
    all_rows = projected.shape[0]
    narrow = heads * key_piece
    broad = heads * value_piece
    query_part = projected[:, :narrow].reshape(all_rows, heads, key_piece)
    key_part = projected[:, narrow : 2 * narrow].reshape(all_rows, heads, key_piece)
    value_part = projected[:, 2 * narrow : 2 * narrow + broad].reshape(all_rows, heads, value_piece)
    outgate_part = projected[:, 2 * narrow + broad :].reshape(all_rows, heads, value_piece)
    query, key, value, outgate = (
        lax.all_to_all(query_part, "ep", split_axis=0, concat_axis=2, tiled=True),
        lax.all_to_all(key_part, "ep", split_axis=0, concat_axis=2, tiled=True),
        lax.all_to_all(value_part, "ep", split_axis=0, concat_axis=2, tiled=True),
        lax.all_to_all(outgate_part, "ep", split_axis=0, concat_axis=2, tiled=True),
    )
    in_pre = product(normed, w_input)
    log_forget = jax.nn.log_sigmoid(product(normed, w_forget) + forget_bias)
    scaled = query.astype(jnp.float32) * key_size ** (-0.5)
    key_heads = key.astype(jnp.float32)
    value_heads = value.astype(jnp.float32)
    stab_next = jnp.maximum(log_forget + stabilizer, in_pre)
    decay = jnp.exp(log_forget + stabilizer - stab_next)
    inweight = jnp.exp(in_pre - stab_next)
    memory_next = decay[:, :, None, None] * memory + inweight[:, :, None, None] * (
        key_heads[:, :, :, None] * value_heads[:, :, None, :]
    )
    normalizer_next = decay[:, :, None] * normalizer + inweight[:, :, None] * key_heads
    numerator = jnp.einsum("shd,shde->she", scaled, memory_next, precision=lax.Precision.HIGHEST)
    denominator = jnp.sum(scaled * normalizer_next, axis=-1)
    hidden = numerator / jnp.maximum(jnp.abs(denominator), jnp.exp(-stab_next))[:, :, None]
    hidden = (
        hidden.reshape(seqs, value_width)
        * jax.nn.sigmoid(outgate.reshape(seqs, value_width).astype(jnp.float32))
    ).astype(jnp.bfloat16)
    partial_value = product(lax.all_gather(hidden, "ep", axis=0, tiled=True), w_out)
    summed = lax.psum(rounded_term(partial_value).astype(jnp.bfloat16), "tp")
    mixed = lax.all_to_all(summed, "ep", split_axis=0, concat_axis=1, tiled=True)
    resid = tokens.astype(jnp.float32) + mixed.astype(jnp.float32)
    ffn_in = rms_scale(resid, ffn_gain).astype(jnp.bfloat16)
    gate_local, up_local, down_local = (w_gate[0], w_up[0], w_down[0])
    n_experts = lax.axis_size("ep") * w_gate.shape[0]
    piece = lax.all_gather(ffn_in, "ep", axis=0, tiled=True)
    gate_part = product(piece, gate_local)
    up_part = product(piece, up_local)
    act = (jax.nn.silu(gate_part) * up_part).astype(jnp.bfloat16)
    expert_terms = rounded_term(product(act, down_local))
    labels = jnp.arange(n_experts, dtype=jnp.int32)
    route_dense = jnp.sum(
        jnp.where(expert_ids[:, :, None] == labels[None, None, :], route_weights[:, :, None], 0.0),
        axis=1,
    )
    my_weight = lax.all_to_all(route_dense, "ep", split_axis=1, concat_axis=0, tiled=True)
    contrib = expert_terms * my_weight
    n_ep = lax.axis_size("ep")
    n_tp = lax.axis_size("tp")
    arranged = jnp.swapaxes(contrib.reshape(n_ep, seqs, n_tp, width // n_tp), 1, 2)
    arranged = arranged.reshape(n_ep * n_tp * seqs, width // n_tp)
    mine = lax.psum_scatter(arranged, ("ep", "tp"), scatter_dimension=0, tiled=True)
    ffn_out = lax.all_gather(mine.astype(jnp.bfloat16), "tp", axis=1, tiled=True).astype(mine.dtype)
    out = (resid + ffn_out).astype(jnp.bfloat16)
    return (out, memory_next, normalizer_next, stab_next)


def solution(mesh):
    return jax.shard_map(
        body,
        mesh=mesh,
        in_specs=(
            P("ep", None),
            P("ep", "tp", None, None),
            P("ep", "tp", None),
            P("ep", "tp"),
            P(),
            P(None, "tp", "ep"),
            P(None, "tp", "ep"),
            P(None, "tp", "ep"),
            P(None, "tp", "ep"),
            P(None, "tp"),
            P(None, "tp"),
            P("tp"),
            P("tp", "ep"),
            P(),
            P("ep", None, "tp"),
            P("ep", None, "tp"),
            P("ep", "tp", None),
            P("ep", None),
            P("ep", None),
        ),
        out_specs=(P("ep", None), P("ep", "tp", None, None), P("ep", "tp", None), P("ep", "tp")),
        check_vma=False,
    )
```

profile of v0, /device:TPU:0, one launch (start us, length us, event | category | flops | bytes accessed | tf_op | source)
XLA Modules:
  0.0 274.0 jit_solution(16929384175384432204)
XLA Ops:
  0.7 1.1 fusion.14
  1.7 0.9 fusion.49
  2.6 45.3 %all-gather = bf16[16,4,4096]{2,1,0:T(4,128)(2,1)S(1)} all-gather(bf16[1,4,4096]{2,1,0:T(4,128)(2,1)S(1)} %fusion.49), channel_id=1, replica_groups=mesh['ep'=16,'tp'=2] {'ep'}, dimensions={0}, use_global_device_ids=true | all-gather | bytes 557056 | tf_op jit(solution)/shard_map/all_gather | solution.py:50
  48.0 1.3 convolution_convert_fusion.4
  49.5 0.1 copy.119
  49.6 0.7 reshape.153
  50.3 3.5 %all-to-all-start.1 = ((bf16[16,2,128]{2,1,0:T(2,128)(2,1)}), bf16[16,2,128]{2,1,0:T(2,128)(2,1)S(1)}, u32[]{:S(2)}, u32[]{:S(2)}) async-start(bf16[16,2,128]{2,1,0:T(2,128)(2,1)} %reshape.153), calls=%async_computation.1 | async-start | bytes 16384 | tf_op jit(solution)/shard_map/all_to_all | solution.py:69
  53.8 0.8 fusion.16
  54.6 0.9 fusion.29
  55.5 0.9 subtract_exponential_fusion.1
  56.5 1.3 convolution_convert_fusion.5
  57.9 1.7 convolution_convert_fusion.3
  59.6 1.7 convolution_convert_fusion.2
  61.3 0.8 select_reduce_fusion
  62.2 0.1 copy.114
  62.3 0.7 reshape.149
  63.1 0.1 copy.123
  63.2 0.7 reshape.151
  64.1 0.1 copy.127
  64.2 0.7 reshape.155
  64.9 0.7 copy.131
  65.6 6.9 %all-to-all-start = ((bf16[16,2,128]{2,1,0:T(2,128)(2,1)}), bf16[16,2,128]{2,1,0:T(2,128)(2,1)S(1)}, u32[]{:S(2)}, u32[]{:S(2)}) async-start(bf16[16,2,128]{2,1,0:T(2,128)(2,1)} %reshape.149), calls=%async_computation | async-start | bytes 16384 | tf_op jit(solution)/shard_map/all_to_all | solution.py:68
  72.7 7.0 %all-to-all-done = bf16[16,2,128]{2,1,0:T(2,128)(2,1)S(1)} async-done(((bf16[16,2,128]{2,1,0:T(2,128)(2,1)}), bf16[16,2,128]{2,1,0:T(2,128)(2,1)S(1)}, u32[]{:S(2)}, u32[]{:S(2)}) %all-to-all-start) | async-done | bytes 8224 | tf_op jit(solution)/shard_map/all_to_all | solution.py:68
  79.7 3.5 %all-to-all-start.2 = ((bf16[16,2,256]{2,1,0:T(2,128)(2,1)}), bf16[16,2,256]{2,1,0:T(2,128)(2,1)S(1)}, u32[]{:S(2)}, u32[]{:S(2)}) async-start(bf16[16,2,256]{2,1,0:T(2,128)(2,1)} %reshape.151), calls=%async_computation.2 | async-start | bytes 32768 | tf_op jit(solution)/shard_map/all_to_all | solution.py:70
  83.6 0.7 multiply_reduce_fusion.1
  84.5 6.1 %all-to-all-done.2 = bf16[16,2,256]{2,1,0:T(2,128)(2,1)S(1)} async-done(((bf16[16,2,256]{2,1,0:T(2,128)(2,1)}), bf16[16,2,256]{2,1,0:T(2,128)(2,1)S(1)}, u32[]{:S(2)}, u32[]{:S(2)}) %all-to-all-start.2) | async-done | bytes 16416 | tf_op jit(solution)/shard_map/all_to_all | solution.py:70
  90.6 3.5 %all-to-all-start.3 = ((bf16[16,2,256]{2,1,0:T(2,128)(2,1)}), bf16[16,2,256]{2,1,0:T(2,128)(2,1)S(1)}, u32[]{:S(2)}, u32[]{:S(2)}) async-start(bf16[16,2,256]{2,1,0:T(2,128)(2,1)} %reshape.155), calls=%async_computation.3 | async-start | bytes 32768 | tf_op jit(solution)/shard_map/all_to_all | solution.py:71
  94.3 4.2 %multiply_add_fusion = f32[4,4,256,512]{3,2,1,0:T(8,128)S(1)} fusion(f32[4,4,256,512]{3,2,1,0:T(8,128)} %param.20, f32[4,4,512]{2,1,0:T(4,128)S(1)} %reshape.121, f32[4,4,256]{2,1,0:T(4,128)S(1)} %reshape.120, f32[4,4]{1,0:T(4,128)S(1)} %subtract_exponential_fusion, f32[4,4]{1,0:T(4,128)S(1)} %get-tuple-element.6), kind=kLoop, calls=%fused_computation | loop fusion | flops 8388608 | bytes 16826496 | tf_op jit(solution)/shard_map/add | solution.py:81
  98.5 3.4 %copy-done.1 = f32[4,4,256,512]{3,2,1,0:T(8,128)} copy-done((f32[4,4,256,512]{3,2,1,0:T(8,128)}, f32[4,4,256,512]{3,2,1,0:T(8,128)S(1)}, u32[]{:S(2)}) %copy-start.1) | copy-done | bytes 8388632
  101.9 4.0 %fusion.30 = f32[4,4,1,512]{3,2,1,0:T(1,128)S(1)} fusion(f32[4,4,256,1]{2,3,1,0:T(1,128)S(1)} %reshape.141, f32[4,4,256,512]{3,2,1,0:T(8,128)S(1)} %multiply_add_fusion), kind=kOutput, calls=%fused_computation.57 | convolution fusion | flops 25165824 | bytes 8437760 | tf_op jit(solution)/shard_map/shd,shde->she/dot_general | solution.py:85
  106.1 6.9 %all-to-all-start.5 = ((f32[4,16,1]{0,2,1:T(1,128)}), f32[4,16,1]{0,2,1:T(1,128)S(1)}, u32[]{:S(2)}, u32[]{:S(2)}) async-start(f32[4,16,1]{0,2,1:T(1,128)} %copy.131), calls=%async_computation.5 | async-start | bytes 16384 | tf_op jit(solution)/shard_map/all_to_all | solution.py:109
  113.5 42.4 %all-gather.1 = bf16[16,4,2048]{2,1,0:T(4,128)(2,1)S(1)} all-gather(bf16[1,4,2048]{2,1,0:T(4,128)(2,1)S(1)} %fusion.25), channel_id=1, replica_groups=mesh['ep'=16,'tp'=2] {'ep'}, dimensions={0}, use_global_device_ids=true | all-gather | bytes 278528 | tf_op jit(solution)/shard_map/all_gather | solution.py:92
  155.8 0.8 reshape.135
  156.6 1.2 convolution_convert_fusion.1
  157.9 4.0 %psum.7 = bf16[16,4,256]{2,1,0:T(4,128)(2,1)} all-reduce(bf16[16,4,256]{2,1,0:T(4,128)(2,1)S(1)} %all_to_all.24), channel_id=1, replica_groups=mesh['ep'=16,'tp'=2] {'tp'}, use_global_device_ids=true, to_apply=%region_2.3 | all-reduce | flops 16384 | bytes 65536 | tf_op jit(solution)/shard_map/psum | solution.py:93
  161.9 3.5 %all-to-all-start.4 = ((bf16[16,4,256]{2,1,0:T(4,128)(2,1)}), bf16[16,4,256]{2,1,0:T(4,128)(2,1)S(1)}, u32[]{:S(2)}, u32[]{:S(2)}) async-start(bf16[16,4,256]{2,1,0:T(4,128)(2,1)} %psum.7), calls=%async_computation.4 | async-start | bytes 65536 | tf_op jit(solution)/shard_map/all_to_all | solution.py:94
  165.5 7.3 %all-to-all-done.4 = bf16[16,4,256]{2,1,0:T(4,128)(2,1)S(1)} async-done(((bf16[16,4,256]{2,1,0:T(4,128)(2,1)}), bf16[16,4,256]{2,1,0:T(4,128)(2,1)S(1)}, u32[]{:S(2)}, u32[]{:S(2)}) %all-to-all-start.4) | async-done | bytes 32800 | tf_op jit(solution)/shard_map/all_to_all | solution.py:94
  172.8 0.1 multiply_reduce_fusion
  173.0 39.4 %all-gather.2 = bf16[16,4,4096]{2,1,0:T(4,128)(2,1)S(1)} all-gather(bf16[1,4,4096]{2,1,0:T(4,128)(2,1)S(1)} %fusion.22), channel_id=1, replica_groups=mesh['ep'=16,'tp'=2] {'ep'}, dimensions={0}, use_global_device_ids=true | all-gather | bytes 557056 | tf_op jit(solution)/shard_map/all_gather | solution.py:99
  212.5 2.0 fusion.3
  214.6 3.8 %convolution_convert_fusion = bf16[64,4096]{1,0:T(8,128)(2,1)} fusion(bf16[1,256,4096]{2,1,0:T(8,128)(2,1)S(1)} %copy-done, bf16[64,4096]{1,0:T(8,128)(2,1)S(1)} %reshape.137, bf16[1,4096,256]{2,1,0:T(8,128)(2,1)} %param.34, f32[64,256]{1,0:T(8,128)S(1)} %fusion.3), kind=kOutput, calls=%fused_computation.1 | convolution fusion | flops 268795904 | bytes 5308416 | tf_op jit(solution)/shard_map/dot_general | solution.py:12
  218.4 1.2 convert_multiply_fusion
  219.6 1.9 reshape.118
  221.4 1.9 copy.132
  223.4 1.3 reshape.119
  224.7 46.8 %all-reduce.2 = bf16[128,2048]{1,0:T(8,128)(2,1)S(1)} all-reduce(f32[128,2048]{1,0:T(8,128)} %reshape.119), channel_id=2, replica_groups=mesh['ep'=16,'tp'=2] {'ep','tp'}, use_global_device_ids=true, to_apply=%region_5.6.clone | all-reduce | flops 262144 | bytes 1572864
  271.5 1.8 all_gather.15
  273.4 0.6 add_convert_fusion
  (58 shorter events, 2.5 us)
Async XLA Ops:
  0.6 214.0 %copy-start = (bf16[1,256,4096]{2,1,0:T(8,128)(2,1)S(1)}, bf16[1,256,4096]{2,1,0:T(8,128)(2,1)}, u32[]{:S(2)}) copy-start(bf16[1,256,4096]{2,1,0:T(8,128)(2,1)} %param.35) | copy-start | bytes 6291460
  0.6 83.0 %copy-start.5 = (f32[4,4,256]{2,1,0:T(4,128)S(1)}, f32[4,4,256]{2,1,0:T(4,128)}, u32[]{:S(2)}) copy-start(f32[4,4,256]{2,1,0:T(4,128)} %param.21) | copy-start | bytes 49156
  50.3 15.3 %all-to-all-start.1 = ((bf16[16,2,128]{2,1,0:T(2,128)(2,1)}), bf16[16,2,128]{2,1,0:T(2,128)(2,1)S(1)}, u32[]{:S(2)}, u32[]{:S(2)}) async-start(bf16[16,2,128]{2,1,0:T(2,128)(2,1)} %reshape.153), calls=%async_computation.1 | async-start | bytes 16384 | tf_op jit(solution)/shard_map/all_to_all | solution.py:69
  56.5 42.0 %copy-start.6 = (f32[4,4]{1,0:T(4,128)}, f32[4,4]{1,0:T(4,128)S(1)}, u32[]{:S(2)}) copy-start(f32[4,4]{1,0:T(4,128)S(1)} %get-tuple-element.7) | copy-start | bytes 196
  65.6 14.1 %all-to-all-start = ((bf16[16,2,128]{2,1,0:T(2,128)(2,1)}), bf16[16,2,128]{2,1,0:T(2,128)(2,1)S(1)}, u32[]{:S(2)}, u32[]{:S(2)}) async-start(bf16[16,2,128]{2,1,0:T(2,128)(2,1)} %reshape.149), calls=%async_computation | async-start | bytes 16384 | tf_op jit(solution)/shard_map/all_to_all | solution.py:68
  79.7 10.9 %all-to-all-start.2 = ((bf16[16,2,256]{2,1,0:T(2,128)(2,1)}), bf16[16,2,256]{2,1,0:T(2,128)(2,1)S(1)}, u32[]{:S(2)}, u32[]{:S(2)}) async-start(bf16[16,2,256]{2,1,0:T(2,128)(2,1)} %reshape.151), calls=%async_computation.2 | async-start | bytes 32768 | tf_op jit(solution)/shard_map/all_to_all | solution.py:70
  90.6 15.5 %all-to-all-start.3 = ((bf16[16,2,256]{2,1,0:T(2,128)(2,1)}), bf16[16,2,256]{2,1,0:T(2,128)(2,1)S(1)}, u32[]{:S(2)}, u32[]{:S(2)}) async-start(bf16[16,2,256]{2,1,0:T(2,128)(2,1)} %reshape.155), calls=%async_computation.3 | async-start | bytes 32768 | tf_op jit(solution)/shard_map/all_to_all | solution.py:71
  98.5 3.4 %copy-start.1 = (f32[4,4,256,512]{3,2,1,0:T(8,128)}, f32[4,4,256,512]{3,2,1,0:T(8,128)S(1)}, u32[]{:S(2)}) copy-start(f32[4,4,256,512]{3,2,1,0:T(8,128)S(1)} %multiply_add_fusion) | copy-start | bytes 25165828
  101.9 54.7 %copy-start.3 = (bf16[2048,256]{1,0:T(8,128)(2,1)S(1)}, bf16[2048,256]{1,0:T(8,128)(2,1)}, u32[]{:S(2)}) copy-start(bf16[2048,256]{1,0:T(8,128)(2,1)} %param.31) | copy-start | bytes 3145732
  101.9 70.8 %copy-start.2 = (bf16[4,4096]{1,0:T(4,128)(2,1)S(1)}, bf16[4,4096]{1,0:T(4,128)(2,1)}, u32[]{:S(2)}) copy-start(bf16[4,4096]{1,0:T(4,128)(2,1)} %param.19) | copy-start | bytes 98308
  101.9 71.0 %copy-start.4 = (f32[4096]{0:T(1024)S(1)}, f32[4096]{0:T(1024)}, u32[]{:S(2)}) copy-start(f32[4096]{0:T(1024)} %param.32) | copy-start | bytes 49156
  106.1 55.8 %all-to-all-start.5 = ((f32[4,16,1]{0,2,1:T(1,128)}), f32[4,16,1]{0,2,1:T(1,128)S(1)}, u32[]{:S(2)}, u32[]{:S(2)}) async-start(f32[4,16,1]{0,2,1:T(1,128)} %copy.131), calls=%async_computation.5 | async-start | bytes 16384 | tf_op jit(solution)/shard_map/all_to_all | solution.py:109
  161.9 10.9 %all-to-all-start.4 = ((bf16[16,4,256]{2,1,0:T(4,128)(2,1)}), bf16[16,4,256]{2,1,0:T(4,128)(2,1)S(1)}, u32[]{:S(2)}, u32[]{:S(2)}) async-start(bf16[16,4,256]{2,1,0:T(4,128)(2,1)} %psum.7), calls=%async_computation.4 | async-start | bytes 65536 | tf_op jit(solution)/shard_map/all_to_all | solution.py:94
where the time goes:
time: 275 us; the launch traced here: 274 us
  blocking collectives  180 us (65%)
  starting transfers between devices  27.7 us (10%)
  waiting for transfers between devices  20.3 us (7%)
  matrix products  19 us (7%)
  local copies, waits for them, and re-layouts  15.6 us (6%)
  other arithmetic  10.7 us (4%)
    unnamed x1, blocking collectives  46.8 us
    all_gather x1, blocking collectives, body(): piece = lax.all_gather(normed, 'ep', axis=0, tiled=True)  45.3 us
    all_gather x1, blocking collectives, body(): lax.all_gather(hidden, 'ep', axis=0, tiled=True)  42.4 us
    all_gather x1, blocking collectives, body(): piece = lax.all_gather(ffn_in, 'ep', axis=0, tiled=True)  39.4 us
    dot_general x9, matrix products, product(): return jnp.dot(left, right, preferred_element_type=jnp.float32)  15 us
    unnamed x26, local copies, waits for them, and re-layouts  7.67 us
    all_to_all x1, waiting for transfers between devices, body(): lax.all_to_all(summed, 'ep', split_axis=0, concat_axis=1, tiled=True)  7.25 us
    all_to_all x1, waiting for transfers between devices, body(): lax.all_to_all(query_part, 'ep', split_axis=0, concat_axis=2, tiled=True)  6.95 us
  transfers between devices with their start and end apart: 6, of which 3 were waited for; matrix products, arithmetic and copies ran while one was open for 9% of the time, Pallas kernels for 0%

commit v1 on v0

--- a/solution.py
+++ b/solution.py
@@ -47,7 +47,24 @@
     value_cols = w_value.reshape(width, heads * value_piece)
     outgate_cols = w_outgate.reshape(width, heads * value_piece)
     normed = rms_scale(tokens.astype(jnp.float32), norm_gain).astype(jnp.bfloat16)
-    piece = lax.all_gather(normed, "ep", axis=0, tiled=True)
+    count, mine_2, rows = (lax.axis_size("ep"), lax.axis_index("ep"), normed.shape[0])
+    forward = [(i, (i + 1) % count) for i in range(count)]
+    downward = [(i, (i - 1) % count) for i in range(count)]
+    out_2 = jnp.zeros((*normed.shape[:0], count * rows, *normed.shape[0 + 1 :]), normed.dtype)
+    out_2 = lax.dynamic_update_slice_in_dim(out_2, normed, mine_2 * rows, axis=0)
+    from_left = from_right = normed
+    half = count // 2
+    for step in range(1, half + 1):
+        from_left = lax.ppermute(from_left, "ep", forward)
+        out_2 = lax.dynamic_update_slice_in_dim(
+            out_2, from_left, (mine_2 - step) % count * rows, axis=0
+        )
+        if step < count - half:
+            from_right = lax.ppermute(from_right, "ep", downward)
+            out_2 = lax.dynamic_update_slice_in_dim(
+                out_2, from_right, (mine_2 + step) % count * rows, axis=0
+            )
+    piece = out_2
     projected = jnp.concatenate(
         [
             product(piece, query_cols),

time: 275 us -> 291 us (1.058)
  blocking collectives: 180 us -> 134 us
  starting transfers between devices: 27.7 us -> 68.7 us
  waiting for transfers between devices: 20.3 us -> 38.4 us
  local copies, waits for them, and re-layouts: 15.6 us -> 18.6 us
    all_gather x1 -> x0, blocking collectives: 45.3 us -> none  [body(): piece = lax.all_gather(normed, 'ep', axis=0, tiled=True)]
    ppermute x0 -> x15, starting transfers between devices: none -> 41 us  [the longest x7 37.9 us: body(): from_right = lax.ppermute(from_right, 'ep', downward)]
    ppermute x0 -> x15, waiting for transfers between devices: none -> 18.2 us  [the longest x8 18.2 us: body(): from_left = lax.ppermute(from_left, 'ep', forward)]
    unnamed x26 -> x23, local copies, waits for them, and re-layouts: 7.67 us -> 6.86 us
  transfers between devices with their start and end apart: 6 -> 21, of which waited for: 3 -> 10; matrix products, arithmetic and copies ran while one was open for 9% -> 8% of each run, Pallas kernels for 0% -> 0%
where the time goes in v1:
time: 291 us; the launch traced here: 290 us
  blocking collectives  134 us (46%)
  starting transfers between devices  68.7 us (24%)
  waiting for transfers between devices  38.4 us (13%)
  local copies, waits for them, and re-layouts  18.6 us (6%)
  matrix products  18.5 us (6%)
  other arithmetic  9.79 us (3%)
    unnamed x1, blocking collectives  46.7 us
    all_gather x1, blocking collectives, body(): lax.all_gather(hidden, 'ep', axis=0, tiled=True)  42.4 us
    all_gather x1, blocking collectives, body(): piece = lax.all_gather(ffn_in, 'ep', axis=0, tiled=True)  39.4 us
    ppermute x7, starting transfers between devices, body(): from_right = lax.ppermute(from_right, 'ep', downward)  37.9 us
    ppermute x8, waiting for transfers between devices, body(): from_left = lax.ppermute(from_left, 'ep', forward)  18.2 us
    dot_general x9, matrix products, product(): return jnp.dot(left, right, preferred_element_type=jnp.float32)  14.5 us
    all_to_all x1, waiting for transfers between devices, body(): lax.all_to_all(summed, 'ep', split_axis=0, concat_axis=1, tiled=True)  7.25 us
    all_to_all x1, waiting for transfers between devices, body(): lax.all_to_all(query_part, 'ep', split_axis=0, concat_axis=2, tiled=True)  6.95 us
  transfers between devices with their start and end apart: 21, of which 10 were waited for; matrix products, arithmetic and copies ran while one was open for 8% of the time, Pallas kernels for 0%

profile of v1, /device:TPU:0, one launch (start us, length us, event | category | flops | bytes accessed | tf_op | source)
XLA Modules:
  0.0 289.8 jit_solution(17343730909525445023)
XLA Ops:
  0.7 1.1 fusion.14
  1.8 0.9 constant_dynamic-update-slice_fusion.15
  2.7 3.0 %collective-permute-start = (bf16[4,4096]{1,0:T(4,128)(2,1)S(1)}, bf16[4,4096]{1,0:T(4,128)(2,1)S(1)}, u32[]{:S(2)}, u32[]{:S(2)}) collective-permute-start(bf16[4,4096]{1,0:T(4,128)(2,1)S(1)} %get-tuple-element.9), channel_id=1, source_target_pairs={{0,2},{2,4},{4,6},{6,8},{8,10},{10,12},{12,14},{14,16},{16,18},{18... | collective-permute-start | bytes 98312 | tf_op jit(solution)/shard_map/ppermute | solution.py:58
  5.7 4.1 %collective-permute-start.1 = (bf16[4,4096]{1,0:T(4,128)(2,1)S(1)}, bf16[4,4096]{1,0:T(4,128)(2,1)S(1)}, u32[]{:S(2)}, u32[]{:S(2)}) collective-permute-start(bf16[4,4096]{1,0:T(4,128)(2,1)S(1)} %get-tuple-element.9), channel_id=1, source_target_pairs={{0,30},{2,0},{4,2},{6,4},{8,6},{10,8},{12,10},{14,12},{16,14},{18,... | collective-permute-start | bytes 98312 | tf_op jit(solution)/shard_map/ppermute | solution.py:63
  9.7 0.9 fusion.30
  10.6 0.9 subtract_exponential_fusion.1
  11.6 0.8 select_reduce_fusion
  13.3 5.6 %collective-permute-start.3 = (bf16[4,4096]{1,0:T(4,128)(2,1)S(1)}, bf16[4,4096]{1,0:T(4,128)(2,1)S(1)}, u32[]{:S(2)}, u32[]{:S(2)}) collective-permute-start(bf16[4,4096]{1,0:T(4,128)(2,1)S(1)} %collective-permute-done.1), channel_id=1, source_target_pairs={{0,30},{2,0},{4,2},{6,4},{8,6},{10,8},{12,10},{14,12},{16,14},{18,... | collective-permute-start | bytes 98312 | tf_op jit(solution)/shard_map/ppermute | solution.py:63
  19.0 1.8 collective-permute-done.2
  20.8 5.6 %collective-permute-start.5 = (bf16[4,4096]{1,0:T(4,128)(2,1)S(1)}, bf16[4,4096]{1,0:T(4,128)(2,1)S(1)}, u32[]{:S(2)}, u32[]{:S(2)}) collective-permute-start(bf16[4,4096]{1,0:T(4,128)(2,1)S(1)} %collective-permute-done.3), channel_id=1, source_target_pairs={{0,30},{2,0},{4,2},{6,4},{8,6},{10,8},{12,10},{14,12},{16,14},{18,... | collective-permute-start | bytes 98312 | tf_op jit(solution)/shard_map/ppermute | solution.py:63
  26.5 1.8 collective-permute-done.4
  28.3 5.6 %collective-permute-start.7 = (bf16[4,4096]{1,0:T(4,128)(2,1)S(1)}, bf16[4,4096]{1,0:T(4,128)(2,1)S(1)}, u32[]{:S(2)}, u32[]{:S(2)}) collective-permute-start(bf16[4,4096]{1,0:T(4,128)(2,1)S(1)} %collective-permute-done.5), channel_id=1, source_target_pairs={{0,30},{2,0},{4,2},{6,4},{8,6},{10,8},{12,10},{14,12},{16,14},{18,... | collective-permute-start | bytes 98312 | tf_op jit(solution)/shard_map/ppermute | solution.py:63
  34.0 1.8 collective-permute-done.6
  35.8 5.6 %collective-permute-start.9 = (bf16[4,4096]{1,0:T(4,128)(2,1)S(1)}, bf16[4,4096]{1,0:T(4,128)(2,1)S(1)}, u32[]{:S(2)}, u32[]{:S(2)}) collective-permute-start(bf16[4,4096]{1,0:T(4,128)(2,1)S(1)} %collective-permute-done.7), channel_id=1, source_target_pairs={{0,30},{2,0},{4,2},{6,4},{8,6},{10,8},{12,10},{14,12},{16,14},{18,... | collective-permute-start | bytes 98312 | tf_op jit(solution)/shard_map/ppermute | solution.py:63
  41.5 1.8 collective-permute-done.8
  43.3 5.6 %collective-permute-start.11 = (bf16[4,4096]{1,0:T(4,128)(2,1)S(1)}, bf16[4,4096]{1,0:T(4,128)(2,1)S(1)}, u32[]{:S(2)}, u32[]{:S(2)}) collective-permute-start(bf16[4,4096]{1,0:T(4,128)(2,1)S(1)} %collective-permute-done.9), channel_id=1, source_target_pairs={{0,30},{2,0},{4,2},{6,4},{8,6},{10,8},{12,10},{14,12},{16,14},{18,... | collective-permute-start | bytes 98312 | tf_op jit(solution)/shard_map/ppermute | solution.py:63
  49.0 1.8 collective-permute-done.10
  50.8 5.8 %collective-permute-start.13 = (bf16[4,4096]{1,0:T(4,128)(2,1)S(1)}, bf16[4,4096]{1,0:T(4,128)(2,1)S(1)}, u32[]{:S(2)}, u32[]{:S(2)}) collective-permute-start(bf16[4,4096]{1,0:T(4,128)(2,1)S(1)} %collective-permute-done.11), channel_id=1, source_target_pairs={{0,30},{2,0},{4,2},{6,4},{8,6},{10,8},{12,10},{14,12},{16,14},{18,... | collective-permute-start | bytes 98312 | tf_op jit(solution)/shard_map/ppermute | solution.py:63
  56.7 1.6 collective-permute-done.12
  58.4 7.4 %collective-permute-done.14 = bf16[4,4096]{1,0:T(4,128)(2,1)S(1)} collective-permute-done((bf16[4,4096]{1,0:T(4,128)(2,1)S(1)}, bf16[4,4096]{1,0:T(4,128)(2,1)S(1)}, u32[]{:S(2)}, u32[]{:S(2)}) %collective-permute-start.14) | collective-permute-done | bytes 32800 | tf_op jit(solution)/shard_map/ppermute | solution.py:58
  65.9 1.3 convolution_convert_fusion.4
  68.1 3.5 %all-to-all-start.1 = ((bf16[16,2,128]{2,1,0:T(2,128)(2,1)}), bf16[16,2,128]{2,1,0:T(2,128)(2,1)S(1)}, u32[]{:S(2)}, u32[]{:S(2)}) async-start(bf16[16,2,128]{2,1,0:T(2,128)(2,1)} %reshape.151), calls=%async_computation.1 | async-start | bytes 16384 | tf_op jit(solution)/shard_map/all_to_all | solution.py:86
  71.6 1.7 convolution_convert_fusion.3
  73.3 1.7 convolution_convert_fusion.2
  75.0 1.3 convolution_convert_fusion.5
  79.2 6.9 %all-to-all-start = ((bf16[16,2,128]{2,1,0:T(2,128)(2,1)}), bf16[16,2,128]{2,1,0:T(2,128)(2,1)S(1)}, u32[]{:S(2)}, u32[]{:S(2)}) async-start(bf16[16,2,128]{2,1,0:T(2,128)(2,1)} %reshape.147), calls=%async_computation | async-start | bytes 16384 | tf_op jit(solution)/shard_map/all_to_all | solution.py:85
  86.4 7.0 %all-to-all-done = bf16[16,2,128]{2,1,0:T(2,128)(2,1)S(1)} async-done(((bf16[16,2,128]{2,1,0:T(2,128)(2,1)}), bf16[16,2,128]{2,1,0:T(2,128)(2,1)S(1)}, u32[]{:S(2)}, u32[]{:S(2)}) %all-to-all-start) | async-done | bytes 8224 | tf_op jit(solution)/shard_map/all_to_all | solution.py:85
  93.3 3.5 %all-to-all-start.2 = ((bf16[16,2,256]{2,1,0:T(2,128)(2,1)}), bf16[16,2,256]{2,1,0:T(2,128)(2,1)S(1)}, u32[]{:S(2)}, u32[]{:S(2)}) async-start(bf16[16,2,256]{2,1,0:T(2,128)(2,1)} %reshape.149), calls=%async_computation.2 | async-start | bytes 32768 | tf_op jit(solution)/shard_map/all_to_all | solution.py:87
  98.1 6.0 %all-to-all-done.2 = bf16[16,2,256]{2,1,0:T(2,128)(2,1)S(1)} async-done(((bf16[16,2,256]{2,1,0:T(2,128)(2,1)}), bf16[16,2,256]{2,1,0:T(2,128)(2,1)S(1)}, u32[]{:S(2)}, u32[]{:S(2)}) %all-to-all-start.2) | async-done | bytes 16416 | tf_op jit(solution)/shard_map/all_to_all | solution.py:87
  104.1 3.5 %all-to-all-start.3 = ((bf16[16,2,256]{2,1,0:T(2,128)(2,1)}), bf16[16,2,256]{2,1,0:T(2,128)(2,1)S(1)}, u32[]{:S(2)}, u32[]{:S(2)}) async-start(bf16[16,2,256]{2,1,0:T(2,128)(2,1)} %reshape.153), calls=%async_computation.3 | async-start | bytes 32768 | tf_op jit(solution)/shard_map/all_to_all | solution.py:88
  107.9 4.2 %multiply_add_fusion = f32[4,4,256,512]{3,2,1,0:T(8,128)S(1)} fusion(f32[4,4,256,512]{3,2,1,0:T(8,128)} %param.20, f32[4,4,512]{2,1,0:T(4,128)S(1)} %reshape.121, f32[4,4,256]{2,1,0:T(4,128)S(1)} %reshape.120, f32[4,4]{1,0:T(4,128)S(1)} %subtract_exponential_fusion, f32[4,4]{1,0:T(4,128)S(1)} %get-tuple-element.6), kind=kLoop, calls=%fused_computation | loop fusion | flops 8388608 | bytes 16826496 | tf_op jit(solution)/shard_map/add | solution.py:98
  112.1 3.4 %copy-done.1 = f32[4,4,256,512]{3,2,1,0:T(8,128)} copy-done((f32[4,4,256,512]{3,2,1,0:T(8,128)}, f32[4,4,256,512]{3,2,1,0:T(8,128)S(1)}, u32[]{:S(2)}) %copy-start.1) | copy-done | bytes 8388632
  115.5 4.0 %fusion.31 = f32[4,4,1,512]{3,2,1,0:T(1,128)S(1)} fusion(f32[4,4,256,1]{2,3,1,0:T(1,128)S(1)} %reshape.139, f32[4,4,256,512]{3,2,1,0:T(8,128)S(1)} %multiply_add_fusion), kind=kOutput, calls=%fused_computation.73 | convolution fusion | flops 25165824 | bytes 8437760 | tf_op jit(solution)/shard_map/shd,shde->she/dot_general | solution.py:102
  119.7 6.9 %all-to-all-start.5 = ((f32[4,16,1]{0,2,1:T(1,128)}), f32[4,16,1]{0,2,1:T(1,128)S(1)}, u32[]{:S(2)}, u32[]{:S(2)}) async-start(f32[4,16,1]{0,2,1:T(1,128)} %copy.131), calls=%async_computation.5 | async-start | bytes 16384 | tf_op jit(solution)/shard_map/all_to_all | solution.py:126
  127.1 42.4 %all-gather = bf16[16,4,2048]{2,1,0:T(4,128)(2,1)S(1)} all-gather(bf16[1,4,2048]{2,1,0:T(4,128)(2,1)S(1)} %fusion.25), channel_id=1, replica_groups=mesh['ep'=16,'tp'=2] {'ep'}, dimensions={0}, use_global_device_ids=true | all-gather | bytes 278528 | tf_op jit(solution)/shard_map/all_gather | solution.py:109
  169.6 1.5 convolution_convert_fusion.1
  171.1 4.0 %psum.7 = bf16[16,4,256]{2,1,0:T(4,128)(2,1)} all-reduce(bf16[16,4,256]{2,1,0:T(4,128)(2,1)S(1)} %all_to_all.24), channel_id=1, replica_groups=mesh['ep'=16,'tp'=2] {'tp'}, use_global_device_ids=true, to_apply=%region_2.3 | all-reduce | flops 16384 | bytes 65536 | tf_op jit(solution)/shard_map/psum | solution.py:110
  175.1 3.5 %all-to-all-start.4 = ((bf16[16,4,256]{2,1,0:T(4,128)(2,1)}), bf16[16,4,256]{2,1,0:T(4,128)(2,1)S(1)}, u32[]{:S(2)}, u32[]{:S(2)}) async-start(bf16[16,4,256]{2,1,0:T(4,128)(2,1)} %psum.7), calls=%async_computation.4 | async-start | bytes 65536 | tf_op jit(solution)/shard_map/all_to_all | solution.py:111
  178.8 7.3 %all-to-all-done.4 = bf16[16,4,256]{2,1,0:T(4,128)(2,1)S(1)} async-done(((bf16[16,4,256]{2,1,0:T(4,128)(2,1)}), bf16[16,4,256]{2,1,0:T(4,128)(2,1)S(1)}, u32[]{:S(2)}, u32[]{:S(2)}) %all-to-all-start.4) | async-done | bytes 32800 | tf_op jit(solution)/shard_map/all_to_all | solution.py:111
  186.3 39.4 %all-gather.1 = bf16[16,4,4096]{2,1,0:T(4,128)(2,1)S(1)} all-gather(bf16[1,4,4096]{2,1,0:T(4,128)(2,1)S(1)} %fusion.22), channel_id=1, replica_groups=mesh['ep'=16,'tp'=2] {'ep'}, dimensions={0}, use_global_device_ids=true | all-gather | bytes 557056 | tf_op jit(solution)/shard_map/all_gather | solution.py:116
  225.8 2.1 fusion.3
  227.9 3.0 %convolution_convert_fusion = bf16[64,4096]{1,0:T(8,128)(2,1)S(1)} fusion(bf16[1,256,4096]{2,1,0:T(8,128)(2,1)S(1)} %copy-done, bf16[64,4096]{1,0:T(8,128)(2,1)S(1)} %reshape.135, bf16[1,4096,256]{2,1,0:T(8,128)(2,1)} %param.34, f32[64,256]{1,0:T(8,128)S(1)} %fusion.3), kind=kOutput, calls=%fused_computation.1 | convolution fusion | flops 268795904 | bytes 5308416 | tf_op jit(solution)/shard_map/dot_general | solution.py:12
  230.9 1.1 convert_multiply_fusion
  232.0 3.1 %reshape.118 = f32[16,4,2,2048]{3,2,1,0:T(2,128)} reshape(f32[64,4096]{1,0:T(8,128)} %convert_multiply_fusion) | data formatting | bytes 2097152 | tf_op jit(solution)/shard_map/reshape | solution.py:130
  235.1 2.9 %copy.132 = f32[16,2,4,2048]{3,2,1,0:T(4,128)} copy(f32[16,2,4,2048]{3,1,2,0:T(2,128)} %bitcast.83) | data formatting | bytes 2097152 | tf_op jit(solution)/shard_map/transpose | solution.py:130
  238.0 2.6 reshape.119
  240.6 46.7 %all-reduce.2 = bf16[128,2048]{1,0:T(8,128)(2,1)S(1)} all-reduce(f32[128,2048]{1,0:T(8,128)} %reshape.119), channel_id=2, replica_groups=mesh['ep'=16,'tp'=2] {'ep','tp'}, use_global_device_ids=true, to_apply=%region_5.6.clone | all-reduce | flops 262144 | bytes 1572864
  287.4 1.8 all_gather.11
  (99 shorter events, 8.5 us)
Async XLA Ops:
  0.6 227.2 %copy-start = (bf16[1,256,4096]{2,1,0:T(8,128)(2,1)S(1)}, bf16[1,256,4096]{2,1,0:T(8,128)(2,1)}, u32[]{:S(2)}) copy-start(bf16[1,256,4096]{2,1,0:T(8,128)(2,1)} %param.35) | copy-start | bytes 6291460
  0.6 96.6 %copy-start.4 = (f32[4,4,256]{2,1,0:T(4,128)S(1)}, f32[4,4,256]{2,1,0:T(4,128)}, u32[]{:S(2)}) copy-start(f32[4,4,256]{2,1,0:T(4,128)} %param.21) | copy-start | bytes 49156
  2.7 10.6 %collective-permute-start = (bf16[4,4096]{1,0:T(4,128)(2,1)S(1)}, bf16[4,4096]{1,0:T(4,128)(2,1)S(1)}, u32[]{:S(2)}, u32[]{:S(2)}) collective-permute-start(bf16[4,4096]{1,0:T(4,128)(2,1)S(1)} %get-tuple-element.9), channel_id=1, source_target_pairs={{0,2},{2,4},{4,6},{6,8},{8,10},{10,12},{12,14},{14,16},{16,18},{18... | collective-permute-start | bytes 98312 | tf_op jit(solution)/shard_map/ppermute | solution.py:58
  5.7 7.6 %collective-permute-start.1 = (bf16[4,4096]{1,0:T(4,128)(2,1)S(1)}, bf16[4,4096]{1,0:T(4,128)(2,1)S(1)}, u32[]{:S(2)}, u32[]{:S(2)}) collective-permute-start(bf16[4,4096]{1,0:T(4,128)(2,1)S(1)} %get-tuple-element.9), channel_id=1, source_target_pairs={{0,30},{2,0},{4,2},{6,4},{8,6},{10,8},{12,10},{14,12},{16,14},{18,... | collective-permute-start | bytes 98312 | tf_op jit(solution)/shard_map/ppermute | solution.py:63
  11.6 100.5 %copy-start.5 = (f32[4,4]{1,0:T(4,128)}, f32[4,4]{1,0:T(4,128)S(1)}, u32[]{:S(2)}) copy-start(f32[4,4]{1,0:T(4,128)S(1)} %get-tuple-element.7) | copy-start | bytes 196
  13.3 7.5 %collective-permute-start.2 = (bf16[4,4096]{1,0:T(4,128)(2,1)S(1)}, bf16[4,4096]{1,0:T(4,128)(2,1)S(1)}, u32[]{:S(2)}, u32[]{:S(2)}) collective-permute-start(bf16[4,4096]{1,0:T(4,128)(2,1)S(1)} %collective-permute-done), channel_id=1, source_target_pairs={{0,2},{2,4},{4,6},{6,8},{8,10},{10,12},{12,14},{14,16},{16,18},{18... | collective-permute-start | bytes 98312 | tf_op jit(solution)/shard_map/ppermute | solution.py:58
  13.3 7.5 %collective-permute-start.3 = (bf16[4,4096]{1,0:T(4,128)(2,1)S(1)}, bf16[4,4096]{1,0:T(4,128)(2,1)S(1)}, u32[]{:S(2)}, u32[]{:S(2)}) collective-permute-start(bf16[4,4096]{1,0:T(4,128)(2,1)S(1)} %collective-permute-done.1), channel_id=1, source_target_pairs={{0,30},{2,0},{4,2},{6,4},{8,6},{10,8},{12,10},{14,12},{16,14},{18,... | collective-permute-start | bytes 98312 | tf_op jit(solution)/shard_map/ppermute | solution.py:63
  20.8 7.5 %collective-permute-start.4 = (bf16[4,4096]{1,0:T(4,128)(2,1)S(1)}, bf16[4,4096]{1,0:T(4,128)(2,1)S(1)}, u32[]{:S(2)}, u32[]{:S(2)}) collective-permute-start(bf16[4,4096]{1,0:T(4,128)(2,1)S(1)} %collective-permute-done.2), channel_id=1, source_target_pairs={{0,2},{2,4},{4,6},{6,8},{8,10},{10,12},{12,14},{14,16},{16,18},{18... | collective-permute-start | bytes 98312 | tf_op jit(solution)/shard_map/ppermute | solution.py:58
  20.8 7.5 %collective-permute-start.5 = (bf16[4,4096]{1,0:T(4,128)(2,1)S(1)}, bf16[4,4096]{1,0:T(4,128)(2,1)S(1)}, u32[]{:S(2)}, u32[]{:S(2)}) collective-permute-start(bf16[4,4096]{1,0:T(4,128)(2,1)S(1)} %collective-permute-done.3), channel_id=1, source_target_pairs={{0,30},{2,0},{4,2},{6,4},{8,6},{10,8},{12,10},{14,12},{16,14},{18,... | collective-permute-start | bytes 98312 | tf_op jit(solution)/shard_map/ppermute | solution.py:63
  28.3 7.5 %collective-permute-start.6 = (bf16[4,4096]{1,0:T(4,128)(2,1)S(1)}, bf16[4,4096]{1,0:T(4,128)(2,1)S(1)}, u32[]{:S(2)}, u32[]{:S(2)}) collective-permute-start(bf16[4,4096]{1,0:T(4,128)(2,1)S(1)} %collective-permute-done.4), channel_id=1, source_target_pairs={{0,2},{2,4},{4,6},{6,8},{8,10},{10,12},{12,14},{14,16},{16,18},{18... | collective-permute-start | bytes 98312 | tf_op jit(solution)/shard_map/ppermute | solution.py:58
  28.3 7.5 %collective-permute-start.7 = (bf16[4,4096]{1,0:T(4,128)(2,1)S(1)}, bf16[4,4096]{1,0:T(4,128)(2,1)S(1)}, u32[]{:S(2)}, u32[]{:S(2)}) collective-permute-start(bf16[4,4096]{1,0:T(4,128)(2,1)S(1)} %collective-permute-done.5), channel_id=1, source_target_pairs={{0,30},{2,0},{4,2},{6,4},{8,6},{10,8},{12,10},{14,12},{16,14},{18,... | collective-permute-start | bytes 98312 | tf_op jit(solution)/shard_map/ppermute | solution.py:63
  35.8 7.5 %collective-permute-start.8 = (bf16[4,4096]{1,0:T(4,128)(2,1)S(1)}, bf16[4,4096]{1,0:T(4,128)(2,1)S(1)}, u32[]{:S(2)}, u32[]{:S(2)}) collective-permute-start(bf16[4,4096]{1,0:T(4,128)(2,1)S(1)} %collective-permute-done.6), channel_id=1, source_target_pairs={{0,2},{2,4},{4,6},{6,8},{8,10},{10,12},{12,14},{14,16},{16,18},{18... | collective-permute-start | bytes 98312 | tf_op jit(solution)/shard_map/ppermute | solution.py:58
  35.8 7.5 %collective-permute-start.9 = (bf16[4,4096]{1,0:T(4,128)(2,1)S(1)}, bf16[4,4096]{1,0:T(4,128)(2,1)S(1)}, u32[]{:S(2)}, u32[]{:S(2)}) collective-permute-start(bf16[4,4096]{1,0:T(4,128)(2,1)S(1)} %collective-permute-done.7), channel_id=1, source_target_pairs={{0,30},{2,0},{4,2},{6,4},{8,6},{10,8},{12,10},{14,12},{16,14},{18,... | collective-permute-start | bytes 98312 | tf_op jit(solution)/shard_map/ppermute | solution.py:63
  43.3 7.5 %collective-permute-start.10 = (bf16[4,4096]{1,0:T(4,128)(2,1)S(1)}, bf16[4,4096]{1,0:T(4,128)(2,1)S(1)}, u32[]{:S(2)}, u32[]{:S(2)}) collective-permute-start(bf16[4,4096]{1,0:T(4,128)(2,1)S(1)} %collective-permute-done.8), channel_id=1, source_target_pairs={{0,2},{2,4},{4,6},{6,8},{8,10},{10,12},{12,14},{14,16},{16,18},{18... | collective-permute-start | bytes 98312 | tf_op jit(solution)/shard_map/ppermute | solution.py:58
  43.3 7.5 %collective-permute-start.11 = (bf16[4,4096]{1,0:T(4,128)(2,1)S(1)}, bf16[4,4096]{1,0:T(4,128)(2,1)S(1)}, u32[]{:S(2)}, u32[]{:S(2)}) collective-permute-start(bf16[4,4096]{1,0:T(4,128)(2,1)S(1)} %collective-permute-done.9), channel_id=1, source_target_pairs={{0,30},{2,0},{4,2},{6,4},{8,6},{10,8},{12,10},{14,12},{16,14},{18,... | collective-permute-start | bytes 98312 | tf_op jit(solution)/shard_map/ppermute | solution.py:63
  50.8 7.5 %collective-permute-start.12 = (bf16[4,4096]{1,0:T(4,128)(2,1)S(1)}, bf16[4,4096]{1,0:T(4,128)(2,1)S(1)}, u32[]{:S(2)}, u32[]{:S(2)}) collective-permute-start(bf16[4,4096]{1,0:T(4,128)(2,1)S(1)} %collective-permute-done.10), channel_id=1, source_target_pairs={{0,2},{2,4},{4,6},{6,8},{8,10},{10,12},{12,14},{14,16},{16,18},{18... | collective-permute-start | bytes 98312 | tf_op jit(solution)/shard_map/ppermute | solution.py:58
  50.8 7.5 %collective-permute-start.13 = (bf16[4,4096]{1,0:T(4,128)(2,1)S(1)}, bf16[4,4096]{1,0:T(4,128)(2,1)S(1)}, u32[]{:S(2)}, u32[]{:S(2)}) collective-permute-start(bf16[4,4096]{1,0:T(4,128)(2,1)S(1)} %collective-permute-done.11), channel_id=1, source_target_pairs={{0,30},{2,0},{4,2},{6,4},{8,6},{10,8},{12,10},{14,12},{16,14},{18,... | collective-permute-start | bytes 98312 | tf_op jit(solution)/shard_map/ppermute | solution.py:63
  58.3 7.5 %collective-permute-start.14 = (bf16[4,4096]{1,0:T(4,128)(2,1)S(1)}, bf16[4,4096]{1,0:T(4,128)(2,1)S(1)}, u32[]{:S(2)}, u32[]{:S(2)}) collective-permute-start(bf16[4,4096]{1,0:T(4,128)(2,1)S(1)} %collective-permute-done.12), channel_id=1, source_target_pairs={{0,2},{2,4},{4,6},{6,8},{8,10},{10,12},{12,14},{14,16},{16,18},{18... | collective-permute-start | bytes 98312 | tf_op jit(solution)/shard_map/ppermute | solution.py:58
  68.1 11.1 %all-to-all-start.1 = ((bf16[16,2,128]{2,1,0:T(2,128)(2,1)}), bf16[16,2,128]{2,1,0:T(2,128)(2,1)S(1)}, u32[]{:S(2)}, u32[]{:S(2)}) async-start(bf16[16,2,128]{2,1,0:T(2,128)(2,1)} %reshape.151), calls=%async_computation.1 | async-start | bytes 16384 | tf_op jit(solution)/shard_map/all_to_all | solution.py:86
  79.2 14.1 %all-to-all-start = ((bf16[16,2,128]{2,1,0:T(2,128)(2,1)}), bf16[16,2,128]{2,1,0:T(2,128)(2,1)S(1)}, u32[]{:S(2)}, u32[]{:S(2)}) async-start(bf16[16,2,128]{2,1,0:T(2,128)(2,1)} %reshape.147), calls=%async_computation | async-start | bytes 16384 | tf_op jit(solution)/shard_map/all_to_all | solution.py:85
  93.3 10.8 %all-to-all-start.2 = ((bf16[16,2,256]{2,1,0:T(2,128)(2,1)}), bf16[16,2,256]{2,1,0:T(2,128)(2,1)S(1)}, u32[]{:S(2)}, u32[]{:S(2)}) async-start(bf16[16,2,256]{2,1,0:T(2,128)(2,1)} %reshape.149), calls=%async_computation.2 | async-start | bytes 32768 | tf_op jit(solution)/shard_map/all_to_all | solution.py:87
  104.1 15.5 %all-to-all-start.3 = ((bf16[16,2,256]{2,1,0:T(2,128)(2,1)}), bf16[16,2,256]{2,1,0:T(2,128)(2,1)S(1)}, u32[]{:S(2)}, u32[]{:S(2)}) async-start(bf16[16,2,256]{2,1,0:T(2,128)(2,1)} %reshape.153), calls=%async_computation.3 | async-start | bytes 32768 | tf_op jit(solution)/shard_map/all_to_all | solution.py:88
  112.1 3.4 %copy-start.1 = (f32[4,4,256,512]{3,2,1,0:T(8,128)}, f32[4,4,256,512]{3,2,1,0:T(8,128)S(1)}, u32[]{:S(2)}) copy-start(f32[4,4,256,512]{3,2,1,0:T(8,128)S(1)} %multiply_add_fusion) | copy-start | bytes 25165828
  115.5 70.5 %copy-start.2 = (bf16[4,4096]{1,0:T(4,128)(2,1)S(1)}, bf16[4,4096]{1,0:T(4,128)(2,1)}, u32[]{:S(2)}) copy-start(bf16[4,4096]{1,0:T(4,128)(2,1)} %param.19) | copy-start | bytes 98308
  115.5 70.7 %copy-start.3 = (f32[4096]{0:T(1024)S(1)}, f32[4096]{0:T(1024)}, u32[]{:S(2)}) copy-start(f32[4096]{0:T(1024)} %param.32) | copy-start | bytes 49156
  119.7 55.5 %all-to-all-start.5 = ((f32[4,16,1]{0,2,1:T(1,128)}), f32[4,16,1]{0,2,1:T(1,128)S(1)}, u32[]{:S(2)}, u32[]{:S(2)}) async-start(f32[4,16,1]{0,2,1:T(1,128)} %copy.131), calls=%async_computation.5 | async-start | bytes 16384 | tf_op jit(solution)/shard_map/all_to_all | solution.py:126
  175.1 10.9 %all-to-all-start.4 = ((bf16[16,4,256]{2,1,0:T(4,128)(2,1)}), bf16[16,4,256]{2,1,0:T(4,128)(2,1)S(1)}, u32[]{:S(2)}, u32[]{:S(2)}) async-start(bf16[16,4,256]{2,1,0:T(4,128)(2,1)} %psum.7), calls=%async_computation.4 | async-start | bytes 65536 | tf_op jit(solution)/shard_map/all_to_all | solution.py:111
